TPU v7x, 256 devices: a 4x2x16 block of a 4x16x16 slice. The times are simulated.
256 devices in a mesh: grp: 2 (over y), ep: 32 (over z, core), tp: 4 (over x).
Axes of the slice: x: 4, y: 2, z: 16, core: 2. Of those that a mesh axis runs over, the one named last changes fastest.
The devices are a block of a 4x16x16 slice.
Arguments:
- queries: bfloat16 [24576, 1024], P(('grp', 'ep'), 'tp'), parts along dimension 0, may hold values from -6 to 6
- key_values: bfloat16 [24576, 512], P(('grp', 'ep'), 'tp'), parts along dimension 0, may hold values from -6 to 6
- query_gain: float32 [64], replicated, may hold values from 0.5 to 5
- key_gain: float32 [64], replicated, may hold values from 0.5 to 5
- out_weight: bfloat16 [1024, 2048], P('tp'), may hold values from -0.1875 to 0.1875
- second_batch: bfloat16 [32768, 2048], P(('grp', 'ep', 'tp')), parts along dimension 0, may hold values from -6 to 6
- norm_gain: float32 [2048], replicated, may hold values from 0.1 to 1.9
- routes: int32 [32768, 2], P(('grp', 'ep', 'tp')), parts along dimension 0, may hold values from 0 to 63, all different within a row; in each aligned block of 128 rows (0 to 127, 128 to 255, ...) at most 6 rows name the same one
- route_weights: float32 [32768, 2], P(('grp', 'ep', 'tp')), parts along dimension 0, may hold values from 0.2 to 1
- expert_gate: bfloat16 [64, 2048, 1024], P('ep', None, 'tp'), may hold values from -0.125 to 0.125
- expert_up: bfloat16 [64, 2048, 1024], P('ep', None, 'tp'), may hold values from -0.125 to 0.125
- expert_down: bfloat16 [64, 1024, 2048], P('ep', 'tp'), may hold values from -0.1875 to 0.1875
- shared_gate: bfloat16 [2048, 512], P(None, 'tp'), may hold values from -0.125 to 0.125
- shared_up: bfloat16 [2048, 512], P(None, 'tp'), may hold values from -0.125 to 0.125
- shared_down: bfloat16 [512, 2048], P('tp'), may hold values from -0.25 to 0.25
Outputs:
- mixer_out: bfloat16 [24576, 2048], P(('grp', 'ep', 'tp')), parts along dimension 0
- channel_out: bfloat16 [32768, 2048], P(('grp', 'ep', 'tp')), parts along dimension 0
There are 2 independent parts, one for each index of `grp`. A program takes and returns all parts, laid end to end along the dimension named above; an argument that names none is the same for every part. Nothing has to cross between parts.
Inputs may be any that keep to these rules, and one draw needn't show every extreme that they name: `routes`: each row names 2 different experts. Among the rows of one device no expert is named more than 6 times, and in every draw some expert is named exactly 6 times by the rows of some device.
All inputs are finite; a program needn't handle non-finite values.
Results may differ from a plain program's by a relative error of at most 0.015.
The roundings to bfloat16 on the way count: a program that leaves them out, or rounds other values in their place, can miss the bound.
Values may be sent and summed in bfloat16 or wider, within the bound.
A program may use at most 128 MiB of HBM per device.

v0:
```python
import jax
import jax.numpy as jnp
from jax import lax
from jax.sharding import Mesh
from jax.sharding import PartitionSpec as P

GRID_W = 64
EP = ("ep_0", "ep_1")
GRP_EP = ("grp", "ep_0", "ep_1")
GRP_EP_TP = ("grp", "ep_0", "ep_1", "tp")
rope_base = 10000.0
norm_eps = 1e-06


def joined_along(tiles, dim):
    shape = list(tiles.shape[1:])
    shape[dim] *= tiles.shape[0]
    return jnp.moveaxis(tiles, 0, dim).reshape(shape)


def stacked_from(shard, axes, order):
    tiles = shard
    for k in order:
        tiles = lax.all_gather(tiles, axes[k])
    done = order[::-1]
    back = [done.index(k) for k in range(len(axes))]
    tiles = tiles.transpose(*back, *range(len(axes), tiles.ndim))
    return tiles.reshape(-1, *shard.shape)


def whole_of(shard, axes, order, dim):
    return joined_along(stacked_from(shard, axes, order), dim)


def from_everyone(shard, axis):
    copies = jnp.broadcast_to(shard, (lax.axis_size(axis), *shard.shape))
    return lax.all_to_all(copies, axis, split_axis=0, concat_axis=0, tiled=True)


def gathered_copies(shard, axis, dim):
    return joined_along(from_everyone(shard, axis), dim)


def in_blocks(shard, dim, length):
    shape = shard.shape
    tiles = shard.reshape(*shape[:dim], length, shape[dim] // length, *shape[dim + 1 :])
    return jnp.moveaxis(tiles, dim, 0)


def summed_on_arrival(shard, axis, dim):
    tiles = in_blocks(shard, dim, lax.axis_size(axis))
    arrived = lax.all_to_all(tiles, axis, split_axis=0, concat_axis=0, tiled=True)
    return arrived.astype(jnp.float32).sum(axis=0)


def head_norm(vectors, gain):
    return (
        vectors * lax.rsqrt(jnp.mean(vectors * vectors, axis=-1, keepdims=True) + norm_eps) * gain
    )


def turn_heads(vectors, positions):
    row_count, head_count, head_size = vectors.shape
    half_size = head_size // 2
    inverse = rope_base ** (-jnp.arange(0, half_size, 2, dtype=jnp.float32) / half_size)
    grid_row = (positions // GRID_W).astype(jnp.float32)
    grid_column = (positions % GRID_W).astype(jnp.float32)
    angles = jnp.concatenate([grid_row[:, None] * inverse, grid_column[:, None] * inverse], axis=-1)
    cosine = jnp.cos(angles)[:, None, :]
    sine = jnp.sin(angles)[:, None, :]
    paired = vectors.reshape(row_count, head_count, half_size, 2)
    first = paired[..., 0]
    second = paired[..., 1]
    turned = jnp.stack([first * cosine - second * sine, first * sine + second * cosine], axis=-1)
    return turned.reshape(vectors.shape)


def slot_ids(route_rows, expert_count, capacity):
    row_count, top_count = route_rows.shape
    flat_routes = route_rows.reshape(-1)
    onehot = (flat_routes[:, None] == jnp.arange(expert_count, dtype=jnp.int32)[None, :]).astype(
        jnp.int32
    )
    earlier = jnp.cumsum(onehot, axis=0) - onehot
    within = jnp.sum(earlier * onehot, axis=1)
    return (flat_routes * capacity + within).reshape(row_count, top_count)


def slot_table(slots, slot_count):
    row_count, top_count = slots.shape
    flat_slots = slots.reshape(-1)
    owner_row = jnp.arange(row_count * top_count, dtype=jnp.int32) // top_count
    matches = flat_slots[None, :] == jnp.arange(slot_count, dtype=jnp.int32)[:, None]
    occupied = jnp.any(matches, axis=1)
    source_row = jnp.sum(jnp.where(matches, owner_row[None, :], 0), axis=1)
    return jnp.where(occupied, source_row, row_count)


def pick_block(row_count):
    for candidate in range(min(row_count, 1024), 0, -1):
        if row_count % candidate == 0:
            return candidate
    return row_count


def attend_keys(query_turned, scale, running, pieces):
    head_size = query_turned.shape[-1]
    key_block = pick_block(pieces.shape[0])
    blocks = pieces.reshape(pieces.shape[0] // key_block, key_block, 2 * head_size)

    def one_block(carried, block_rows):
        top_now, total_now, acc_now = carried
        scores = (
            jnp.einsum(
                "qhd,kd->hqk",
                query_turned,
                block_rows[:, :head_size],
                preferred_element_type=jnp.float32,
            )
            * scale
        )
        top_new = jnp.maximum(top_now, jnp.max(scores, axis=-1))
        shrink = jnp.exp(top_now - top_new)
        exps = jnp.exp(scores - top_new[..., None])
        total_new = total_now * shrink + jnp.sum(exps, axis=-1)
        acc_new = acc_now * shrink[..., None] + jnp.einsum(
            "hqk,kd->hqd",
            exps.astype(jnp.bfloat16),
            block_rows[:, head_size:],
            preferred_element_type=jnp.float32,
        )
        return ((top_new, total_new, acc_new), None)

    result, ignored = lax.scan(one_block, running, blocks)
    return result


def shared_hidden_of(token_rows, gate_weights, up_weights):
    gate_part = jnp.dot(token_rows, gate_weights, preferred_element_type=jnp.float32)
    up_part = jnp.dot(token_rows, up_weights, preferred_element_type=jnp.float32)
    return (jax.nn.silu(gate_part) * up_part).astype(jnp.bfloat16)


def expert_hidden(slot_rows, gate_weights, up_weights):
    gate_part = jnp.einsum(
        "osjcd,jdf->osjcf", slot_rows, gate_weights, preferred_element_type=jnp.float32
    )
    up_part = jnp.einsum(
        "osjcd,jdf->osjcf", slot_rows, up_weights, preferred_element_type=jnp.float32
    )
    return (jax.nn.silu(gate_part) * up_part).astype(jnp.bfloat16)


def body(
    queries,
    key_values,
    query_gain,
    key_gain,
    out_weight,
    second_batch,
    norm_gain,
    routes,
    route_weights,
    expert_gate,
    expert_up,
    expert_down,
    shared_gate,
    shared_up,
    shared_down,
):
    query_rows = queries.shape[0]
    head_size = query_gain.shape[0]
    heads_here = queries.shape[1] // head_size
    ep_count = lax.axis_size(EP)
    positions = lax.axis_index(EP) * query_rows + jnp.arange(query_rows, dtype=jnp.int32)
    query_turned = turn_heads(
        head_norm(
            queries.reshape(query_rows, heads_here, head_size).astype(jnp.float32), query_gain
        ),
        positions,
    ).astype(jnp.bfloat16)
    key_turned = turn_heads(
        head_norm(key_values[:, None, :head_size].astype(jnp.float32), key_gain), positions
    ).astype(jnp.bfloat16)
    keys_and_values = jnp.concatenate([key_turned[:, 0, :], key_values[:, head_size:]], axis=1)
    start_state = (
        jnp.full((heads_here, query_rows), -1e30, jnp.float32),
        jnp.zeros((heads_here, query_rows), jnp.float32),
        jnp.zeros((heads_here, query_rows, head_size), jnp.float32),
    )
    top_all, total_all, acc_all = attend_keys(
        query_turned, head_size ** (-0.5), start_state, whole_of(keys_and_values, EP, (0, 1), 0)
    )
    head_out = (
        (acc_all / total_all[..., None])
        .transpose(1, 0, 2)
        .reshape(query_rows, heads_here * head_size)
        .astype(jnp.bfloat16)
    )
    tok_count = second_batch.shape[0]
    model_width = second_batch.shape[1]
    top_count = routes.shape[1]
    local_experts = expert_gate.shape[0]
    expert_count = local_experts * ep_count
    capacity = 3 * tok_count * top_count // (2 * expert_count)
    slot_count = expert_count * capacity
    token_float = second_batch.astype(jnp.float32)
    normed = (
        token_float
        * lax.rsqrt(jnp.mean(token_float * token_float, axis=-1, keepdims=True) + norm_eps)
        * norm_gain
    ).astype(jnp.bfloat16)
    own_slots = slot_ids(routes, expert_count, capacity)
    shared_hidden = (lambda pieces, begin_at: shared_hidden_of(pieces, shared_gate, shared_up))(
        gathered_copies(normed, "tp", 0), jnp.int32(0)
    )
    outgoing = jnp.take(
        normed, slot_table(own_slots, slot_count), axis=0, mode="fill", fill_value=0
    )[None]
    arrived = lax.all_to_all(outgoing, EP, split_axis=1, concat_axis=1, tiled=True)
    arrived = arrived.reshape(arrived.shape[0], ep_count, local_experts, capacity, model_width)
    hidden = expert_hidden(
        lax.all_gather(arrived, "tp", axis=0, tiled=True), expert_gate, expert_up
    )
    routed_part = jnp.einsum(
        "osjcf,jfd->osjcd", hidden, expert_down, preferred_element_type=jnp.float32
    ).reshape(-1, model_width)
    shared_part = jnp.dot(shared_hidden, shared_down, preferred_element_type=jnp.float32)
    head_partial = jnp.dot(head_out, out_weight, preferred_element_type=jnp.float32)
    attn_sum, routed_sum, shared_sum = (
        summed_on_arrival(head_partial.astype(jnp.bfloat16), "tp", 0),
        summed_on_arrival(routed_part.astype(jnp.bfloat16), "tp", 0),
        summed_on_arrival(shared_part.astype(jnp.bfloat16), "tp", 0),
    )
    returned = lax.all_to_all(
        routed_sum.astype(jnp.bfloat16), EP, split_axis=0, concat_axis=0, tiled=True
    )
    combined = shared_sum
    for slot_pick in range(top_count):
        combined = combined + route_weights[:, slot_pick : slot_pick + 1] * jnp.take(
            returned, own_slots[:, slot_pick], axis=0
        ).astype(jnp.float32)
    return (attn_sum.astype(jnp.bfloat16), combined.astype(jnp.bfloat16))


def solution(mesh):
    torus = Mesh(
        mesh.devices.reshape(mesh.shape["grp"], 16, 2, mesh.shape["tp"]),
        ("grp", "ep_0", "ep_1", "tp"),
    )
    return jax.shard_map(
        body,
        mesh=torus,
        in_specs=(
            P(GRP_EP, "tp"),
            P(GRP_EP, "tp"),
            P(),
            P(),
            P("tp", None),
            P(GRP_EP_TP, None),
            P(),
            P(GRP_EP_TP, None),
            P(GRP_EP_TP, None),
            P(EP, None, "tp"),
            P(EP, None, "tp"),
            P(EP, "tp", None),
            P(None, "tp"),
            P(None, "tp"),
            P("tp", None),
        ),
        out_specs=(P(GRP_EP_TP, None), P(GRP_EP_TP, None)),
        check_vma=False,
    )
```

profile of v0, /device:TPU:33, one launch (start us, length us, event | category | flops | bytes accessed | tf_op | source)
XLA Modules:
  0.0 621.9 jit_solution(13244901644372939689)
XLA Ops:
  17.1 4.1 copy.120
  21.7 12.4 %reduce.10 = bf16[384,2048]{1,0:T(8,128)(2,1)} reduce(bf16[384,1,2048]{2,1,0:T(2,128)(2,1)} %bitcast.152, bf16[]{:T(256)} %broadcast.416), dimensions={1}, to_apply=%bitcast.134.reduce_sub_computation | reduce | bytes 3145730
  34.1 5.2 reshape.492
  39.3 25.6 %all-to-all-start.3 = ((bf16[32,2,12288]{2,1,0:T(2,128)(2,1)}), bf16[32,2,12288]{2,1,0:T(2,128)(2,1)}, u32[]{:S(2)}, u32[]{:S(2)}) async-start(bf16[32,2,12288]{2,1,0:T(2,128)(2,1)} %reshape.492), calls=%async_computation.3 | async-start | bytes 3145728 | tf_op jit(solution)/shard_map/all_to_all | solution.py:220
  66.8 95.3 %all-gather.8.cloned.1.call-done = bf16[6144,128]{0,1:T(8,128)(2,1)} async-done(((bf16[384,128]{0,1:T(8,128)(2,1)}), bf16[6144,128]{0,1:T(8,128)(2,1)}) %all-gather.8.cloned.1.call-update) | async-done | bytes 1572880 | tf_op jit(solution)/shard_map/all_gather | solution.py:24
  164.9 9.5 %reshape.493 = bf16[384,1,2048]{2,1,0:T(2,128)(2,1)} reshape(bf16[32,2,12288]{2,1,0:T(2,128)(2,1)} %all-to-all-done.3) | data formatting | bytes 3145728
  174.3 12.2 %bitcast_reduce_fusion.2 = bf16[384,2048]{1,0:T(8,128)(2,1)} fusion(bf16[384,1,2048]{2,1,0:T(2,128)(2,1)} %reshape.493), kind=kLoop, calls=%fused_computation.129 | loop fusion | bytes 3145728 | tf_op jit(solution)/shard_map/all_to_all | solution.py:220
  195.7 4.8 all-to-all-start.1
  202.6 25.4 %all-to-all-done.1 = bf16[4,128,2048]{2,1,0:T(8,128)(2,1)} async-done(((bf16[4,128,2048]{2,1,0:T(8,128)(2,1)}), bf16[4,128,2048]{2,1,0:T(8,128)(2,1)}, u32[]{:S(2)}, u32[]{:S(2)}) %all-to-all-start.1) | async-done | bytes 2097184 | tf_op jit(solution)/shard_map/all_to_all | solution.py:37
  230.3 5.5 convolution_convert_fusion
  235.8 4.5 all-to-all-start.2
  244.4 55.9 %all-gather.6.cloned.1.call-done = bf16[4,32,2,6,2048]{4,1,3,0,2:T(8,128)(2,1)} async-done(((bf16[1,32,2,6,2048]{4,1,3,0,2:T(8,128)(2,1)}), bf16[4,32,2,6,2048]{4,1,3,0,2:T(8,128)(2,1)}) %all-gather.6.cloned.1.call-update) | async-done | bytes 6291472 | tf_op jit(solution)/shard_map/all_gather | solution.py:223
  300.3 6.4 %fusion.14 = f32[2,4,32,6,256]{4,2,3,1,0:T(8,128)} fusion(bf16[4,32,2,6,2048]{4,1,3,0,2:T(8,128)(2,1)} %all-gather.6.cloned.1.call-done, bf16[2,2048,256]{2,1,0:T(8,128)(2,1)} %param.28), kind=kOutput, calls=%fused_computation.27 | convolution fusion | flops 1610612736 | bytes 9961472 | tf_op jit(solution)/shard_map/osjcd,jdf->osjcf/dot_general | solution.py:145
  306.7 10.1 %convert_bitcast_fusion = bf16[4,32,2,6,2048]{4,1,3,0,2:T(8,128)(2,1)} fusion(bf16[2,256,2048]{2,1,0:T(8,128)(2,1)S(1)} %copy-done, f32[2,4,32,6,256]{4,2,3,1,0:T(8,128)} %fusion.14, bf16[4,32,2,6,2048]{4,1,3,0,2:T(8,128)(2,1)} %all-gather.6.cloned.1.call-done, bf16[2,2048,256]{2,1,0:T(8,128)(2,1)} %param.29), kind=kOutput, calls=%fused_computation.20 | convolution fusion | flops 3226730496 | bytes 18350080 | tf_op jit(solution)/shard_map/osjcf,jfd->osjcd/dot_general | solution.py:225
  316.8 10.2 %copy.100 = bf16[4,32,2,6,2048]{4,0,3,2,1:T(4,128)(2,1)} copy(bf16[4,32,2,6,2048]{4,1,3,0,2:T(8,128)(2,1)} %convert_bitcast_fusion) | data formatting | bytes 12582912 | tf_op jit(solution)/shard_map/convert_element_type | solution.py:232
  327.0 9.1 %copy.101 = bf16[4,384,2048]{2,1,0:T(8,128)(2,1)} copy(bf16[4,384,2048]{2,0,1:T(4,128)(2,1)} %bitcast.151) | data formatting | bytes 12582912 | tf_op jit(solution)/shard_map/convert_element_type | solution.py:232
  336.1 5.3 all-to-all-start.4
  341.5 127.8 %while.15 = (s32[]{:T(128)}, f32[4,384]{1,0:T(4,128)S(1)}, f32[4,384]{1,0:T(4,128)S(1)}, f32[4,384,64]{1,2,0:T(8,128)S(1)}, bf16[12,1024,128]{2,1,0:T(8,128)(2,1...) while((s32[]{:T(128)}, f32[4,384]{1,0:T(4,128)S(1)}, f32[4,384]{1,0:T(4,128)S(1)}, ...), condition=%wide.region_5.6_spmd.clone, body=%wide.region_2.5_spmd.clone.sunk | while | flops 415538688 | bytes 46432384 | solution.py:134
  346.3 4.0 fusion.76
  357.0 4.0 fusion.76
  367.6 4.0 fusion.76
  378.2 4.0 fusion.76
  399.5 4.0 fusion.76
  420.8 4.0 fusion.76
  442.1 4.0 fusion.76
  463.4 4.0 fusion.76
  471.1 4.1 all-to-all-start
  475.3 5.7 reduce_sum.96
  484.5 10.4 %all-to-all-done = bf16[4,96,2048]{2,1,0:T(8,128)(2,1)S(1)} async-done(((bf16[4,96,2048]{2,1,0:T(8,128)(2,1)}), bf16[4,96,2048]{2,1,0:T(8,128)(2,1)S(1)}, u32[]{:S(2)}, u32[]{:S(2)}) %all-to-all-start) | async-done | bytes 1572896 | tf_op jit(solution)/shard_map/all_to_all | solution.py:52
  495.0 11.2 %all-to-all-start.5 = ((bf16[32,12,2048]{2,1,0:T(8,128)(2,1)}), bf16[32,12,2048]{2,1,0:T(8,128)(2,1)}, u32[]{:S(2)}, u32[]{:S(2)}) async-start(bf16[32,12,2048]{2,1,0:T(8,128)(2,1)} %all_to_all.28), calls=%async_computation.5 | async-start | bytes 4194304 | tf_op jit(solution)/shard_map/all_to_all | solution.py:235
  509.6 94.8 %all-to-all-done.5 = bf16[32,12,2048]{2,1,0:T(8,128)(2,1)} async-done(((bf16[32,12,2048]{2,1,0:T(8,128)(2,1)}), bf16[32,12,2048]{2,1,0:T(8,128)(2,1)}, u32[]{:S(2)}, u32[]{:S(2)}) %all-to-all-start.5) | async-done | bytes 1572896 | tf_op jit(solution)/shard_map/all_to_all | solution.py:235
  608.7 4.0 gather_fusion.2
  (212 shorter events, 143.3 us)
Async XLA Ops:
  7.2 299.5 %copy-start = (bf16[2,256,2048]{2,1,0:T(8,128)(2,1)S(1)}, bf16[2,256,2048]{2,1,0:T(8,128)(2,1)}, u32[]{:S(2)}) copy-start(bf16[2,256,2048]{2,1,0:T(8,128)(2,1)} %param.30) | copy-start | bytes 6291460
  39.3 25.7 %copy-start.5 = (bf16[384,128]{1,0:T(8,128)(2,1)S(1)}, bf16[384,128]{1,0:T(8,128)(2,1)}, u32[]{:S(2)}) copy-start(bf16[384,128]{1,0:T(8,128)(2,1)} %param.20) | copy-start | bytes 294916
  39.3 26.0 %copy-start.9 = (f32[64]{0:T(128)S(1)}, f32[64]{0:T(128)}, u32[]{:S(2)}) copy-start(f32[64]{0:T(128)} %param.22) | copy-start | bytes 772
  39.3 125.6 %all-to-all-start.3 = ((bf16[32,2,12288]{2,1,0:T(2,128)(2,1)}), bf16[32,2,12288]{2,1,0:T(2,128)(2,1)}, u32[]{:S(2)}, u32[]{:S(2)}) async-start(bf16[32,2,12288]{2,1,0:T(2,128)(2,1)} %reshape.492), calls=%async_computation.3 | async-start | bytes 3145728 | tf_op jit(solution)/shard_map/all_to_all | solution.py:220
  64.9 97.2 %all-gather.8.cloned.1.call-start = ((), (), s32[]{:S(2)}) async-start(), calls=%async_computation.7 | async-start | bytes 1671168 | tf_op jit(solution)/shard_map/all_gather | solution.py:24
  66.7 173.7 %all-gather.10.cloned.1.call-start = ((), (), s32[]{:S(2)}) async-start(), calls=%async_computation.8 | async-start | bytes 4718592 | tf_op jit(solution)/shard_map/all_gather | solution.py:24
  164.8 135.5 %all-gather.6.cloned.1.call-start = ((), (), s32[]{:S(2)}) async-start(), calls=%async_computation.6 | async-start | bytes 7864320 | tf_op jit(solution)/shard_map/all_gather | solution.py:223
  195.7 4.9 copy-start.6
  195.7 5.3 copy-start.10
  195.7 32.2 %all-to-all-start.1 = ((bf16[4,128,2048]{2,1,0:T(8,128)(2,1)}), bf16[4,128,2048]{2,1,0:T(8,128)(2,1)}, u32[]{:S(2)}, u32[]{:S(2)}) async-start(bf16[4,128,2048]{2,1,0:T(8,128)(2,1)} %broadcast_in_dim.47), calls=%async_computation.1 | async-start | bytes 4194304 | tf_op jit(solution)/shard_map/all_to_all | solution.py:37
  235.8 100.3 %all-to-all-start.2 = ((bf16[4,128,2048]{2,1,0:T(8,128)(2,1)}), bf16[4,128,2048]{2,1,0:T(8,128)(2,1)}, u32[]{:S(2)}, u32[]{:S(2)}) async-start(bf16[4,128,2048]{2,1,0:T(8,128)(2,1)} %bitcast.153), calls=%async_computation.2 | async-start | bytes 4194304 | tf_op jit(solution)/shard_map/all_to_all | solution.py:52
  336.1 135.0 %all-to-all-start.4 = ((bf16[4,384,2048]{2,1,0:T(8,128)(2,1)}), bf16[4,384,2048]{2,1,0:T(8,128)(2,1)}, u32[]{:S(2)}, u32[]{:S(2)}) async-start(bf16[4,384,2048]{2,1,0:T(8,128)(2,1)} %copy.101), calls=%async_computation.4 | async-start | bytes 12582912 | tf_op jit(solution)/shard_map/all_to_all | solution.py:52
  341.4 127.9 %copy-start.4 = (bf16[256,2048]{1,0:T(8,128)(2,1)S(1)}, bf16[256,2048]{1,0:T(8,128)(2,1)}, u32[]{:S(2)}) copy-start(bf16[256,2048]{1,0:T(8,128)(2,1)} %param.23) | copy-start | bytes 3145732
  346.3 4.6 copy-start.2
  357.0 4.6 copy-start.2
  367.6 4.6 copy-start.2
  378.2 4.6 copy-start.2
  388.9 4.6 copy-start.2
  399.5 4.6 copy-start.2
  410.2 4.6 copy-start.2
  420.8 4.6 copy-start.2
  431.5 4.6 copy-start.2
  442.1 4.6 copy-start.2
  452.7 4.6 copy-start.2
  463.4 4.6 copy-start.2
  471.1 23.9 %all-to-all-start = ((bf16[4,96,2048]{2,1,0:T(8,128)(2,1)}), bf16[4,96,2048]{2,1,0:T(8,128)(2,1)S(1)}, u32[]{:S(2)}, u32[]{:S(2)}) async-start(bf16[4,96,2048]{2,1,0:T(8,128)(2,1)} %bitcast.156), calls=%async_computation | async-start | bytes 3145728 | tf_op jit(solution)/shard_map/all_to_all | solution.py:52
  484.5 21.8 %copy-start.7 = (s32[128,2]{0,1:T(2,128)S(1)}, s32[128,2]{0,1:T(2,128)}, u32[]{:S(2)}) copy-start(s32[128,2]{0,1:T(2,128)} %param.26) | copy-start | bytes 3076
  484.5 21.9 %copy-start.8 = (f32[128,2]{0,1:T(2,128)S(1)}, f32[128,2]{0,1:T(2,128)}, u32[]{:S(2)}) copy-start(f32[128,2]{0,1:T(2,128)} %param.27) | copy-start | bytes 3076
  495.0 109.4 %all-to-all-start.5 = ((bf16[32,12,2048]{2,1,0:T(8,128)(2,1)}), bf16[32,12,2048]{2,1,0:T(8,128)(2,1)}, u32[]{:S(2)}, u32[]{:S(2)}) async-start(bf16[32,12,2048]{2,1,0:T(8,128)(2,1)} %all_to_all.28), calls=%async_computation.5 | async-start | bytes 4194304 | tf_op jit(solution)/shard_map/all_to_all | solution.py:235
  606.9 1.8 copy-start.3
  608.7 6.4 %copy-start.1 = (bf16[2,256,2048]{2,1,0:T(8,128)(2,1)S(1)}, bf16[2,256,2048]{2,1,0:T(8,128)(2,1)}, u32[]{:S(2)}) copy-start(bf16[2,256,2048]{2,1,0:T(8,128)(2,1)} %param.30) | copy-start | bytes 6291460
Sparse Core Ops, SparseCore 0:
  68.1 93.9 all-gather.7
  164.9 24.2 all-gather.9
  194.1 106.1 all-gather.5
where the time goes:
time: 626 us; the launch traced here: 622 us
  waiting for transfers between devices  282 us (45%)
  local copies, waits for them, and re-layouts  105 us (17%)
  matrix products  84.7 us (14%)
  other arithmetic  79.3 us (13%)
  starting transfers between devices  55.8 us (9%)
  between operations  14.5 us (2%)
    all_gather x2, waiting for transfers between devices, stacked_from(): tiles = lax.all_gather(tiles, axes[k])  95.4 us
    all_to_all x1, waiting for transfers between devices, body(): lax.all_to_all(routed_sum.astype(jnp.bfloat16), EP, split_axis=0, concat_...  94.8 us
    all_gather x1, waiting for transfers between devices, body(): lax.all_gather(arrived, 'tp', axis=0, tiled=True)  55.9 us
    reduce_sum x12, other arithmetic, one_block(): total_new = total_now * shrink + jnp.sum(exps, axis=-1)  47.6 us
    dot_general x12, matrix products, one_block(): jnp.einsum('qhd,kd->hqk', query_turned, block_rows[:, :head_size], prefer...  43.5 us
    all_to_all x1, starting transfers between devices, body(): lax.all_to_all(outgoing, EP, split_axis=1, concat_axis=1, tiled=True)  25.6 us
    all_to_all x1, waiting for transfers between devices, from_everyone(): return lax.all_to_all(copies, axis, split_axis=0, concat_axis=0, tiled=True)  25.4 us
    convert_element_type x2, local copies, waits for them, and re-layouts, body(): routed_part.astype(jnp.bfloat16)  19.3 us
  transfers between devices with their start and end apart: 9, of which 5 were waited for; matrix products, arithmetic and copies ran while one was open for 35% of the time, Pallas kernels for 0%

commit v1 on v0

--- a/solution.py
+++ b/solution.py
@@ -220,7 +220,17 @@
     arrived = lax.all_to_all(outgoing, EP, split_axis=1, concat_axis=1, tiled=True)
     arrived = arrived.reshape(arrived.shape[0], ep_count, local_experts, capacity, model_width)
     hidden = expert_hidden(
-        lax.all_gather(arrived, "tp", axis=0, tiled=True), expert_gate, expert_up
+        jnp.concatenate(
+            lax.all_to_all(
+                jnp.stack([arrived for _ in range(lax.psum(1, "tp"))], 0),
+                axis_name="tp",
+                split_axis=0,
+                concat_axis=0,
+            ),
+            0,
+        ),
+        expert_gate,
+        expert_up,
     )
     routed_part = jnp.einsum(
         "osjcf,jfd->osjcd", hidden, expert_down, preferred_element_type=jnp.float32

time: 626 us -> 589 us (0.941)
  waiting for transfers between devices: 282 us -> 238 us
    all_to_all x1, waiting for transfers between devices: 0.01 us -> 77 us  [body(): lax.all_to_all(outgoing, EP, split_axis=1, concat_axis=1, tiled=True)]
    all_gather x2, waiting for transfers between devices: 95.4 us -> 35 us  [stacked_from(): tiles = lax.all_gather(tiles, axes[k])]
    all_gather x1 -> x0, waiting for transfers between devices: 55.9 us -> none  [body(): lax.all_gather(arrived, 'tp', axis=0, tiled=True)]
    all_to_all x1, waiting for transfers between devices: 25.4 us -> 0.01 us  [from_everyone(): return lax.all_to_all(copies, axis, split_axis=0, concat_axis=0, tiled=True)]
    all_to_all x0 -> x1, waiting for transfers between devices: none -> 19.2 us  [body(): lax.all_to_all(jnp.stack([arrived for _ in range(lax.psum(1, 'tp'))], 0),...]
    another operation x1 -> x4, local copies, waits for them, and re-layouts: 0.01 us -> 12.6 us  [the longest x3 12.6 us: body(): jnp.stack([arrived for _ in range(lax.psum(1, 'tp'))], 0)]
    reshape x2 -> x0, local copies, waits for them, and re-layouts: 7.34 us -> none  [body(): arrived.reshape(arrived.shape[0], ep_count, local_experts, capacity, mode...]
  transfers between devices with their start and end apart: 9 -> 9, of which waited for: 5 -> 6; matrix products, arithmetic and copies ran while one was open for 35% -> 37% of each run, Pallas kernels for 0% -> 0%
where the time goes in v1:
time: 589 us; the launch traced here: 584 us
  waiting for transfers between devices  238 us (40%)
  local copies, waits for them, and re-layouts  110 us (19%)
  matrix products  84.7 us (14%)
  other arithmetic  79.3 us (13%)
  starting transfers between devices  57.1 us (10%)
  between operations  14.7 us (2%)
    all_to_all x1, waiting for transfers between devices, body(): lax.all_to_all(routed_sum.astype(jnp.bfloat16), EP, split_axis=0, concat_...  96.8 us
    all_to_all x1, waiting for transfers between devices, body(): lax.all_to_all(outgoing, EP, split_axis=1, concat_axis=1, tiled=True)  77 us
    reduce_sum x12, other arithmetic, one_block(): total_new = total_now * shrink + jnp.sum(exps, axis=-1)  47.6 us
    dot_general x12, matrix products, one_block(): jnp.einsum('qhd,kd->hqk', query_turned, block_rows[:, :head_size], prefer...  43.5 us
    all_gather x2, waiting for transfers between devices, stacked_from(): tiles = lax.all_gather(tiles, axes[k])  35 us
    all_to_all x1, starting transfers between devices, body(): lax.all_to_all(outgoing, EP, split_axis=1, concat_axis=1, tiled=True)  25.6 us
    convert_element_type x2, local copies, waits for them, and re-layouts, body(): routed_part.astype(jnp.bfloat16)  19.3 us
    all_to_all x1, waiting for transfers between devices, body(): lax.all_to_all(jnp.stack([arrived for _ in range(lax.psum(1, 'tp'))], 0),...  19.2 us
  transfers between devices with their start and end apart: 9, of which 6 were waited for; matrix products, arithmetic and copies ran while one was open for 37% of the time, Pallas kernels for 0%

profile of v1, /device:TPU:33, one launch (start us, length us, event | category | flops | bytes accessed | tf_op | source)
XLA Modules:
  0.0 584.1 jit_solution(6906188248415132187)
XLA Ops:
  17.1 4.1 copy.136
  21.7 12.4 %reduce.10 = bf16[384,2048]{1,0:T(8,128)(2,1)} reduce(bf16[384,1,2048]{2,1,0:T(2,128)(2,1)} %bitcast.159, bf16[]{:T(256)} %broadcast.418), dimensions={1}, to_apply=%bitcast.141.reduce_sub_computation | reduce | bytes 3145730
  34.1 5.0 reshape.496
  39.1 25.6 %all-to-all-start.3 = ((bf16[32,2,12288]{2,1,0:T(2,128)(2,1)}), bf16[32,2,12288]{2,1,0:T(2,128)(2,1)}, u32[]{:S(2)}, u32[]{:S(2)}) async-start(bf16[32,2,12288]{2,1,0:T(2,128)(2,1)} %reshape.496), calls=%async_computation.3 | async-start | bytes 3145728 | tf_op jit(solution)/shard_map/all_to_all | solution.py:220
  65.5 77.0 %all-to-all-done.3 = bf16[32,2,12288]{2,1,0:T(2,128)(2,1)} async-done(((bf16[32,2,12288]{2,1,0:T(2,128)(2,1)}), bf16[32,2,12288]{2,1,0:T(2,128)(2,1)}, u32[]{:S(2)}, u32[]{:S(2)}) %all-to-all-start.3) | async-done | bytes 1572896 | tf_op jit(solution)/shard_map/all_to_all | solution.py:220
  144.2 4.5 all-to-all-start.1
  149.7 9.5 %reshape.497 = bf16[384,1,2048]{2,1,0:T(2,128)(2,1)} reshape(bf16[32,2,12288]{2,1,0:T(2,128)(2,1)} %all-to-all-done.3) | data formatting | bytes 3145728
  159.2 12.2 %bitcast_reduce_fusion.2 = bf16[384,2048]{1,0:T(8,128)(2,1)} fusion(bf16[384,1,2048]{2,1,0:T(2,128)(2,1)} %reshape.497), kind=kLoop, calls=%fused_computation.133 | loop fusion | bytes 3145728 | tf_op jit(solution)/shard_map/all_to_all | solution.py:220
  171.5 4.1 stack_reshape.2
  179.2 4.9 stack.17
  184.1 5.3 all-to-all-start.4
  189.5 16.3 %all-gather.5.cloned.1.call-done = bf16[6144,128]{0,1:T(8,128)(2,1)} async-done(((bf16[384,128]{0,1:T(8,128)(2,1)}), bf16[6144,128]{0,1:T(8,128)(2,1)}) %all-gather.5.cloned.1.call-update) | async-done | bytes 1572880 | tf_op jit(solution)/shard_map/all_gather | solution.py:24
  212.9 5.5 convolution_convert_fusion
  218.4 18.7 %all-gather.7.cloned.1.call-done = bf16[32,384,128]{2,1,0:T(8,128)(2,1)} async-done(((bf16[16,384,128]{2,1,0:T(8,128)(2,1)}), bf16[32,384,128]{2,1,0:T(8,128)(2,1)}) %all-gather.7.cloned.1.call-update) | async-done | bytes 3145744 | tf_op jit(solution)/shard_map/all_gather | solution.py:24
  241.0 19.2 %all-to-all-done.4 = bf16[4,1,32,2,6,2048]{5,2,4,3,1,0:T(8,128)(2,1)} async-done(((bf16[4,1,32,2,6,2048]{5,2,4,3,1,0:T(8,128)(2,1)}), bf16[4,1,32,2,6,2048]{5,2,4,3,1,0:T(8,128)(2,1)}, u32[]{:S(2)}, u32[]{:S(2)}) %all-to-all-start.4) | async-done | bytes 6291488 | tf_op jit(solution)/shard_map/all_to_all | solution.py:224
  260.2 4.7 all-to-all-start.2
  265.0 6.4 %fusion.13 = f32[2,4,32,6,256]{4,2,3,1,0:T(8,128)} fusion(bf16[4,1,32,2,6,2048]{5,2,4,3,1,0:T(8,128)(2,1)} %all-to-all-done.4, bf16[2,2048,256]{2,1,0:T(8,128)(2,1)} %param.28), kind=kOutput, calls=%fused_computation.22 | convolution fusion | flops 1610612736 | bytes 9961472 | tf_op jit(solution)/shard_map/osjcd,jdf->osjcf/dot_general | solution.py:145
  271.4 10.1 %convert_bitcast_fusion = bf16[4,32,2,6,2048]{4,1,3,0,2:T(8,128)(2,1)} fusion(bf16[2,256,2048]{2,1,0:T(8,128)(2,1)S(1)} %copy-done, f32[2,4,32,6,256]{4,2,3,1,0:T(8,128)} %fusion.13, bf16[2,2048,256]{2,1,0:T(8,128)(2,1)} %param.29, bf16[4,1,32,2,6,2048]{5,2,4,3,1,0:T(8,128)(2,1)} %all-to-all-done.4), kind=kOutput, calls=%fused_computation.24 | convolution fusion | flops 3226730496 | bytes 18350080 | tf_op jit(solution)/shard_map/osjcf,jfd->osjcd/dot_general | solution.py:235
  281.4 10.2 %copy.104 = bf16[4,32,2,6,2048]{4,0,3,2,1:T(4,128)(2,1)} copy(bf16[4,32,2,6,2048]{4,1,3,0,2:T(8,128)(2,1)} %convert_bitcast_fusion) | data formatting | bytes 12582912 | tf_op jit(solution)/shard_map/convert_element_type | solution.py:242
  291.7 9.1 %copy.105 = bf16[4,384,2048]{2,1,0:T(8,128)(2,1)} copy(bf16[4,384,2048]{2,0,1:T(4,128)(2,1)} %bitcast.158) | data formatting | bytes 12582912 | tf_op jit(solution)/shard_map/convert_element_type | solution.py:242
  300.8 5.3 all-to-all-start.5
  306.1 127.8 %while.15 = (s32[]{:T(128)}, f32[4,384]{1,0:T(4,128)S(1)}, f32[4,384]{1,0:T(4,128)S(1)}, f32[4,384,64]{1,2,0:T(8,128)S(1)}, bf16[12,1024,128]{2,1,0:T(8,128)(2,1...) while((s32[]{:T(128)}, f32[4,384]{1,0:T(4,128)S(1)}, f32[4,384]{1,0:T(4,128)S(1)}, ...), condition=%wide.region_5.6_spmd.clone, body=%wide.region_2.5_spmd.clone.sunk | while | flops 415538688 | bytes 46432384 | solution.py:134
  311.0 4.0 fusion.82
  364.2 4.0 fusion.82
  385.5 4.0 fusion.82
  406.8 4.0 fusion.82
  435.8 4.1 all-to-all-start
  439.9 5.7 reduce_sum.96
  449.2 9.6 %all-to-all-done = bf16[4,96,2048]{2,1,0:T(8,128)(2,1)S(1)} async-done(((bf16[4,96,2048]{2,1,0:T(8,128)(2,1)}), bf16[4,96,2048]{2,1,0:T(8,128)(2,1)S(1)}, u32[]{:S(2)}, u32[]{:S(2)}) %all-to-all-start) | async-done | bytes 1572896 | tf_op jit(solution)/shard_map/all_to_all | solution.py:52
  458.8 7.3 %all-to-all-start.6 = ((bf16[32,12,2048]{2,1,0:T(8,128)(2,1)}), bf16[32,12,2048]{2,1,0:T(8,128)(2,1)}, u32[]{:S(2)}, u32[]{:S(2)}) async-start(bf16[32,12,2048]{2,1,0:T(8,128)(2,1)} %all_to_all.32), calls=%async_computation.6 | async-start | bytes 4194304 | tf_op jit(solution)/shard_map/all_to_all | solution.py:245
  469.6 96.8 %all-to-all-done.6 = bf16[32,12,2048]{2,1,0:T(8,128)(2,1)} async-done(((bf16[32,12,2048]{2,1,0:T(8,128)(2,1)}), bf16[32,12,2048]{2,1,0:T(8,128)(2,1)}, u32[]{:S(2)}, u32[]{:S(2)}) %all-to-all-start.6) | async-done | bytes 1572896 | tf_op jit(solution)/shard_map/all_to_all | solution.py:245
  570.6 4.0 gather_fusion.2
  (212 shorter events, 155.2 us)
Async XLA Ops:
  7.2 264.2 %copy-start = (bf16[2,256,2048]{2,1,0:T(8,128)(2,1)S(1)}, bf16[2,256,2048]{2,1,0:T(8,128)(2,1)}, u32[]{:S(2)}) copy-start(bf16[2,256,2048]{2,1,0:T(8,128)(2,1)} %param.30) | copy-start | bytes 6291460
  39.1 25.6 %copy-start.5 = (bf16[384,128]{1,0:T(8,128)(2,1)S(1)}, bf16[384,128]{1,0:T(8,128)(2,1)}, u32[]{:S(2)}) copy-start(bf16[384,128]{1,0:T(8,128)(2,1)} %param.20) | copy-start | bytes 294916
  39.1 25.9 %copy-start.9 = (f32[64]{0:T(128)S(1)}, f32[64]{0:T(128)}, u32[]{:S(2)}) copy-start(f32[64]{0:T(128)} %param.22) | copy-start | bytes 772
  39.1 103.5 %all-to-all-start.3 = ((bf16[32,2,12288]{2,1,0:T(2,128)(2,1)}), bf16[32,2,12288]{2,1,0:T(2,128)(2,1)}, u32[]{:S(2)}, u32[]{:S(2)}) async-start(bf16[32,2,12288]{2,1,0:T(2,128)(2,1)} %reshape.496), calls=%async_computation.3 | async-start | bytes 3145728 | tf_op jit(solution)/shard_map/all_to_all | solution.py:220
  144.2 34.9 %all-to-all-start.1 = ((bf16[4,128,2048]{2,1,0:T(8,128)(2,1)}), bf16[4,128,2048]{2,1,0:T(8,128)(2,1)}, u32[]{:S(2)}, u32[]{:S(2)}) async-start(bf16[4,128,2048]{2,1,0:T(8,128)(2,1)} %broadcast_in_dim.47), calls=%async_computation.1 | async-start | bytes 4194304 | tf_op jit(solution)/shard_map/all_to_all | solution.py:37
  148.8 57.0 %all-gather.5.cloned.1.call-start = ((), (), s32[]{:S(2)}) async-start(), calls=%async_computation.7 | async-start | bytes 1671168 | tf_op jit(solution)/shard_map/all_gather | solution.py:24
  184.1 76.2 %all-to-all-start.4 = ((bf16[4,1,32,2,6,2048]{5,2,4,3,1,0:T(8,128)(2,1)}), bf16[4,1,32,2,6,2048]{5,2,4,3,1,0:T(8,128)(2,1)}, u32[]{:S(2)}, u32[]{:S(2)}) async-start(bf16[4,1,32,2,6,2048]{5,2,4,3,1,0:T(8,128)(2,1)} %stack.17), calls=%async_computation.4 | async-start | bytes 12582912 | tf_op jit(solution)/shard_map/all_to_all | solution.py:224
  189.4 19.1 %copy-start.6 = (bf16[384,256]{1,0:T(8,128)(2,1)S(1)}, bf16[384,256]{1,0:T(8,128)(2,1)}, u32[]{:S(2)}) copy-start(bf16[384,256]{1,0:T(8,128)(2,1)} %param.19) | copy-start | bytes 589828
  189.4 19.5 %copy-start.10 = (f32[64]{0:T(128)S(1)}, f32[64]{0:T(128)}, u32[]{:S(2)}) copy-start(f32[64]{0:T(128)} %param.21) | copy-start | bytes 772
  189.4 47.7 %all-gather.7.cloned.1.call-start = ((), (), s32[]{:S(2)}) async-start(), calls=%async_computation.8 | async-start | bytes 4718592 | tf_op jit(solution)/shard_map/all_gather | solution.py:24
  260.2 40.6 %all-to-all-start.2 = ((bf16[4,128,2048]{2,1,0:T(8,128)(2,1)}), bf16[4,128,2048]{2,1,0:T(8,128)(2,1)}, u32[]{:S(2)}, u32[]{:S(2)}) async-start(bf16[4,128,2048]{2,1,0:T(8,128)(2,1)} %bitcast.160), calls=%async_computation.2 | async-start | bytes 4194304 | tf_op jit(solution)/shard_map/all_to_all | solution.py:52
  300.8 135.0 %all-to-all-start.5 = ((bf16[4,384,2048]{2,1,0:T(8,128)(2,1)}), bf16[4,384,2048]{2,1,0:T(8,128)(2,1)}, u32[]{:S(2)}, u32[]{:S(2)}) async-start(bf16[4,384,2048]{2,1,0:T(8,128)(2,1)} %copy.105), calls=%async_computation.5 | async-start | bytes 12582912 | tf_op jit(solution)/shard_map/all_to_all | solution.py:52
  306.1 127.9 %copy-start.4 = (bf16[256,2048]{1,0:T(8,128)(2,1)S(1)}, bf16[256,2048]{1,0:T(8,128)(2,1)}, u32[]{:S(2)}) copy-start(bf16[256,2048]{1,0:T(8,128)(2,1)} %param.23) | copy-start | bytes 3145732
  311.0 4.6 copy-start.2
  321.6 4.6 copy-start.2
  332.3 4.6 copy-start.2
  342.9 4.6 copy-start.2
  353.6 4.6 copy-start.2
  364.2 4.6 copy-start.2
  374.9 4.6 copy-start.2
  385.5 4.6 copy-start.2
  396.1 4.6 copy-start.2
  406.8 4.6 copy-start.2
  417.4 4.6 copy-start.2
  428.1 4.6 copy-start.2
  435.8 23.0 %all-to-all-start = ((bf16[4,96,2048]{2,1,0:T(8,128)(2,1)}), bf16[4,96,2048]{2,1,0:T(8,128)(2,1)S(1)}, u32[]{:S(2)}, u32[]{:S(2)}) async-start(bf16[4,96,2048]{2,1,0:T(8,128)(2,1)} %bitcast.163), calls=%async_computation | async-start | bytes 3145728 | tf_op jit(solution)/shard_map/all_to_all | solution.py:52
  449.2 17.1 %copy-start.7 = (s32[128,2]{0,1:T(2,128)S(1)}, s32[128,2]{0,1:T(2,128)}, u32[]{:S(2)}) copy-start(s32[128,2]{0,1:T(2,128)} %param.26) | copy-start | bytes 3076
  449.2 17.2 %copy-start.8 = (f32[128,2]{0,1:T(2,128)S(1)}, f32[128,2]{0,1:T(2,128)}, u32[]{:S(2)}) copy-start(f32[128,2]{0,1:T(2,128)} %param.27) | copy-start | bytes 3076
  458.8 107.6 %all-to-all-start.6 = ((bf16[32,12,2048]{2,1,0:T(8,128)(2,1)}), bf16[32,12,2048]{2,1,0:T(8,128)(2,1)}, u32[]{:S(2)}, u32[]{:S(2)}) async-start(bf16[32,12,2048]{2,1,0:T(8,128)(2,1)} %all_to_all.32), calls=%async_computation.6 | async-start | bytes 4194304 | tf_op jit(solution)/shard_map/all_to_all | solution.py:245
  568.9 1.8 copy-start.3
  570.6 6.4 %copy-start.1 = (bf16[2,256,2048]{2,1,0:T(8,128)(2,1)S(1)}, bf16[2,256,2048]{2,1,0:T(8,128)(2,1)}, u32[]{:S(2)}) copy-start(bf16[2,256,2048]{2,1,0:T(8,128)(2,1)} %param.30) | copy-start | bytes 6291460
Sparse Core Ops, SparseCore 0:
  152.0 53.7 all-gather.4
  208.6 28.4 all-gather.6
